TPU v7x, 32 devices: a whole 2x2x4 slice. The times are simulated.
32 devices in a mesh: ra: 4 (over y, x), cb: 8 (over z, core).
Axes of the slice: x: 2, y: 2, z: 4, core: 2. Of those that a mesh axis runs over, the one named last changes fastest.
Arguments:
- tokens: bfloat16 [512, 4096], P(None, 'ra'), may hold values from -40 to 40, as said below
- norm_gain: float32 [2, 4096], P(None, 'ra'), may hold values from 0.1 to 1.9
- gate_weight: bfloat16 [2, 4096, 11264], P(None, 'ra', 'cb'), may hold values from -0.09375 to 0.09375
- up_weight: bfloat16 [2, 4096, 11264], P(None, 'ra', 'cb'), may hold values from -0.09375 to 0.09375
- down_weight: bfloat16 [2, 11264, 4096], P(None, 'cb', 'ra'), may hold values from -0.0546875 to 0.0546875
Outputs:
- result: bfloat16 [512, 4096], P(None, 'ra')
Inputs may be any that keep to these rules, and one draw needn't show every extreme that they name: `tokens`: features come in blocks of 32 with scales that differ from block to block by up to a factor of 16.
All inputs are finite; a program needn't handle non-finite values.
Results may differ from a plain program's by a relative error of at most 0.0075.
Values may be sent and summed in bfloat16 or wider, within the bound.
A program may use at most 64 MiB of HBM per device.

v0:
```python
import jax
import jax.numpy as jnp
from jax import lax
from jax.sharding import PartitionSpec as P

D = 4096
LAYERS = 2
epsilon = 1e-06
keep_share = 0.5


def body(tokens, norm_gain, gate_weight, up_weight, down_weight):
    stream = tokens
    for layer in range(LAYERS):
        widened = stream.astype(jnp.float32)
        squares = jnp.sum(widened * widened, axis=1)
        normed = (widened * norm_gain[layer]).astype(jnp.bfloat16)
        gate_part = jnp.dot(normed, gate_weight[layer], preferred_element_type=jnp.float32)
        up_part = jnp.dot(normed, up_weight[layer], preferred_element_type=jnp.float32)
        total = lax.psum(squares, "ra")
        gate_share, up_share = (
            lax.psum_scatter(gate_part, "ra", scatter_dimension=1, tiled=True),
            lax.psum_scatter(up_part, "ra", scatter_dimension=1, tiled=True),
        )
        scale = lax.rsqrt(total / D + epsilon)[:, None]
        share = (jax.nn.silu(gate_share * scale) * (up_share * scale)).astype(jnp.bfloat16)
        hidden = lax.all_gather(share, "ra", axis=1, tiled=True)
        partial_down = jnp.dot(hidden, down_weight[layer], preferred_element_type=jnp.float32)
        branch = lax.psum(partial_down, "cb")
        stream = (keep_share * widened + branch).astype(jnp.bfloat16)
    return stream


def solution(mesh):
    placed = (
        P(None, "ra"),
        P(None, "ra"),
        P(None, "ra", "cb"),
        P(None, "ra", "cb"),
        P(None, "cb", "ra"),
    )
    return jax.shard_map(body, mesh=mesh, in_specs=placed, out_specs=P(None, "ra"), check_vma=False)
```

profile of v0, /device:TPU:0, one launch (start us, length us, event | category | flops | bytes accessed | tf_op | source)
XLA Modules:
  0.0 411.4 jit_solution(7383496427016766130)
XLA Ops:
  6.5 0.0 reduce-scatter.7.cloned.1.call-start
  6.5 0.8 fusion.31
  7.3 5.4 %fusion.8 = f32[512,1408]{0,1:T(8,128)} fusion(bf16[2,1024,1408]{2,1,0:T(8,128)(2,1)} %param.8, bf16[512,1024]{1,0:T(8,128)(2,1)} %param.5, f32[1024]{0:T(1024)S(1)} %bitcast.24), kind=kOutput, calls=%fused_computation.14 | convolution fusion | flops 1477967872 | bytes 6819840 | tf_op jit(solution)/shard_map/dot_general | solution.py:19
  12.7 0.0 copy-start
  12.7 0.0 reduce-scatter.7.cloned.1.call-update
  12.8 0.0 reduce-scatter.5.cloned.1.call-start
  12.8 1.1 copy-done
  14.0 5.1 %fusion.10 = f32[512,1408]{0,1:T(8,128)} fusion(bf16[2,1024,1408]{2,1,0:T(8,128)(2,1)} %param.7, bf16[512,1024]{1,0:T(8,128)(2,1)S(1)} %copy-done, f32[1024]{0:T(1024)S(1)} %bitcast.25), kind=kOutput, calls=%fused_computation.16 | convolution fusion | flops 1477967872 | bytes 6819840 | tf_op jit(solution)/shard_map/dot_general | solution.py:18
  19.1 0.0 reduce-scatter.5.cloned.1.call-update
  19.1 0.0 all-gather.3.cloned.1.call-start
  19.2 0.3 fusion.21
  19.5 11.9 %psum.28 = f32[512]{0:T(512)S(1)} all-reduce(f32[512]{0:T(512)S(1)} %fusion.21), channel_id=1, replica_groups=mesh['ra'=4,'cb'=8] {'ra'}, use_global_device_ids=true, to_apply=%region_2.0 | all-reduce | flops 512 | bytes 4096 | tf_op jit(solution)/shard_map/psum | solution.py:20
  31.4 26.3 %reduce-scatter.7.cloned.1.call-done = f32[512,352]{0,1:T(8,128)} async-done(((f32[512,1408]{0,1:T(8,128)}), f32[512,352]{0,1:T(8,128)}) %reduce-scatter.7.cloned.1.call-update) | async-done | bytes 720912 | tf_op jit(solution)/shard_map/reduce_scatter | solution.py:23
  57.6 44.8 %reduce-scatter.5.cloned.1.call-done = f32[512,352]{0,1:T(8,128)} async-done(((f32[512,1408]{0,1:T(8,128)}), f32[512,352]{0,1:T(8,128)}) %reduce-scatter.5.cloned.1.call-update) | async-done | bytes 720912 | tf_op jit(solution)/shard_map/reduce_scatter | solution.py:22
  102.4 2.3 multiply_convert_fusion.1
  104.7 0.0 all-gather.3.cloned.1.call-update
  104.7 0.0 all-reduce.3.cloned.1.call-start
  104.8 29.8 %all-gather.3.cloned.1.call-done = bf16[512,1408]{0,1:T(8,128)(2,1)} async-done(((bf16[512,352]{0,1:T(8,128)(2,1)}), bf16[512,1408]{0,1:T(8,128)(2,1)}) %all-gather.3.cloned.1.call-update) | async-done | bytes 1441808 | tf_op jit(solution)/shard_map/all_gather | solution.py:27
  134.6 5.4 %fusion.6 = f32[512,1024]{1,0:T(8,128)} fusion(bf16[512,1408]{0,1:T(8,128)(2,1)} %all-gather.3.cloned.1.call-done, bf16[2,1408,1024]{2,1,0:T(8,128)(2,1)} %param.9), kind=kOutput, calls=%fused_computation.12 | convolution fusion | flops 1476395008 | bytes 6422528 | tf_op jit(solution)/shard_map/dot_general | solution.py:28
  140.1 0.0 all-reduce.3.cloned.1.call-update
  140.1 0.0 reduce-scatter.9.cloned.1.call-start
  140.1 65.2 %all-reduce.3.cloned.1.call-done = f32[512,1024]{1,0:T(8,128)} async-done(((f32[512,1024]{1,0:T(8,128)}), f32[512,1024]{1,0:T(8,128)}) %all-reduce.3.cloned.1.call-update) | async-done | bytes 2097168 | tf_op jit(solution)/shard_map/psum | solution.py:29
  205.3 2.0 fusion.25
  207.4 5.1 %fusion.4 = f32[512,1408]{0,1:T(8,128)} fusion(bf16[2,1024,1408]{2,1,0:T(8,128)(2,1)} %param.7, bf16[512,1024]{1,0:T(8,128)(2,1)S(1)} %get-tuple-element.6, f32[1024]{0:T(1024)S(1)} %bitcast.22), kind=kOutput, calls=%fused_computation.10 | convolution fusion | flops 1477967872 | bytes 6819840 | tf_op jit(solution)/shard_map/dot_general | solution.py:18
  212.4 0.0 reduce-scatter.9.cloned.1.call-update
  212.5 0.0 reduce-scatter.11.cloned.1.call-start
  212.5 5.1 %fusion.2 = f32[512,1408]{0,1:T(8,128)} fusion(bf16[2,1024,1408]{2,1,0:T(8,128)(2,1)} %param.8, bf16[512,1024]{1,0:T(8,128)(2,1)S(1)} %get-tuple-element.6, f32[1024]{0:T(1024)S(1)} %bitcast.23), kind=kOutput, calls=%fused_computation.8 | convolution fusion | flops 1477967872 | bytes 6819840 | tf_op jit(solution)/shard_map/dot_general | solution.py:19
  217.7 0.0 reduce-scatter.11.cloned.1.call-update
  217.7 0.0 all-gather.5.cloned.1.call-start
  217.7 10.4 %psum.30 = f32[512]{0:T(512)S(1)} all-reduce(f32[512]{0:T(512)S(1)} %get-tuple-element.5), channel_id=1, replica_groups=mesh['ra'=4,'cb'=8] {'ra'}, use_global_device_ids=true, to_apply=%region_7.8 | all-reduce | flops 512 | bytes 4096 | tf_op jit(solution)/shard_map/psum | solution.py:20
  228.1 26.0 %reduce-scatter.9.cloned.1.call-done = f32[512,352]{0,1:T(8,128)} async-done(((f32[512,1408]{0,1:T(8,128)}), f32[512,352]{0,1:T(8,128)}) %reduce-scatter.9.cloned.1.call-update) | async-done | bytes 720912 | tf_op jit(solution)/shard_map/reduce_scatter | solution.py:22
  254.1 44.7 %reduce-scatter.11.cloned.1.call-done = f32[512,352]{0,1:T(8,128)} async-done(((f32[512,1408]{0,1:T(8,128)}), f32[512,352]{0,1:T(8,128)}) %reduce-scatter.11.cloned.1.call-update) | async-done | bytes 720912 | tf_op jit(solution)/shard_map/reduce_scatter | solution.py:23
  298.8 2.3 multiply_convert_fusion
  301.1 0.0 all-gather.5.cloned.1.call-update
  301.1 0.0 all-reduce.5.cloned.1.call-start
  301.1 29.9 %all-gather.5.cloned.1.call-done = bf16[512,1408]{0,1:T(8,128)(2,1)} async-done(((bf16[512,352]{0,1:T(8,128)(2,1)}), bf16[512,1408]{0,1:T(8,128)(2,1)}) %all-gather.5.cloned.1.call-update) | async-done | bytes 1441808 | tf_op jit(solution)/shard_map/all_gather | solution.py:27
  331.0 5.4 %fusion = f32[512,1024]{1,0:T(8,128)} fusion(bf16[512,1408]{0,1:T(8,128)(2,1)} %all-gather.5.cloned.1.call-done, bf16[2,1408,1024]{2,1,0:T(8,128)(2,1)} %param.9), kind=kOutput, calls=%fused_computation.6 | convolution fusion | flops 1476395008 | bytes 6422528 | tf_op jit(solution)/shard_map/dot_general | solution.py:28
  336.4 0.0 all-reduce.5.cloned.1.call-update
  336.5 65.2 %all-reduce.5.cloned.1.call-done = f32[512,1024]{1,0:T(8,128)} async-done(((f32[512,1024]{1,0:T(8,128)}), f32[512,1024]{1,0:T(8,128)}) %all-reduce.5.cloned.1.call-update) | async-done | bytes 2097168 | tf_op jit(solution)/shard_map/psum | solution.py:29
  401.7 2.9 fusion.23
  (2 shorter events, 0.0 us)
Async XLA Ops:
  6.5 51.1 %reduce-scatter.7.cloned.1.call-start = ((), (), s32[]{:S(2)}) async-start(), calls=%async_computation.5 | async-start | bytes 3604480 | tf_op jit(solution)/shard_map/reduce_scatter | solution.py:23
  12.7 1.2 copy-start
  12.8 89.7 %reduce-scatter.5.cloned.1.call-start = ((), (), s32[]{:S(2)}) async-start(), calls=%async_computation.4 | async-start | bytes 3604480 | tf_op jit(solution)/shard_map/reduce_scatter | solution.py:22
  19.1 115.5 %all-gather.3.cloned.1.call-start = ((), (), s32[]{:S(2)}) async-start(), calls=%async_computation.6 | async-start | bytes 1802240 | tf_op jit(solution)/shard_map/all_gather | solution.py:27
  104.7 100.6 %all-reduce.3.cloned.1.call-start = ((), (), s32[]{:S(2)}) async-start(), calls=%async_computation.7 | async-start | bytes 4194304 | tf_op jit(solution)/shard_map/psum | solution.py:29
  140.1 114.1 %reduce-scatter.9.cloned.1.call-start = ((), (), s32[]{:S(2)}) async-start(), calls=%async_computation.8 | async-start | bytes 3604480 | tf_op jit(solution)/shard_map/reduce_scatter | solution.py:22
  212.5 86.3 %reduce-scatter.11.cloned.1.call-start = ((), (), s32[]{:S(2)}) async-start(), calls=%async_computation.9 | async-start | bytes 3604480 | tf_op jit(solution)/shard_map/reduce_scatter | solution.py:23
  217.7 113.3 %all-gather.5.cloned.1.call-start = ((), (), s32[]{:S(2)}) async-start(), calls=%async_computation.10 | async-start | bytes 1802240 | tf_op jit(solution)/shard_map/all_gather | solution.py:27
  301.1 100.6 %all-reduce.5.cloned.1.call-start = ((), (), s32[]{:S(2)}) async-start(), calls=%async_computation.11 | async-start | bytes 4194304 | tf_op jit(solution)/shard_map/psum | solution.py:29
Sparse Core Ops, SparseCore 0:
  12.9 44.7 reduce-scatter.6
  60.7 41.7 reduce-scatter.4
  104.9 29.7 all-gather.2
  140.2 65.0 all-reduce.2
  212.6 41.4 reduce-scatter.8
  257.0 41.7 reduce-scatter.10
  301.2 29.7 all-gather.4
  336.6 65.0 all-reduce.4
where the time goes:
time: 412 us; the launch traced here: 411 us
  waiting for transfers between devices  332 us (81%)
  matrix products  31.6 us (8%)
  blocking collectives  22.2 us (5%)
  between operations  13.5 us (3%)
  other arithmetic  9.81 us (2%)
    psum x2, waiting for transfers between devices, body(): branch = lax.psum(partial_down, 'cb')  130 us
    reduce_scatter x2, waiting for transfers between devices, body(): lax.psum_scatter(up_part, 'ra', scatter_dimension=1, tiled=True)  70.9 us
    reduce_scatter x2, waiting for transfers between devices, body(): lax.psum_scatter(gate_part, 'ra', scatter_dimension=1, tiled=True)  70.8 us
    all_gather x2, waiting for transfers between devices, body(): hidden = lax.all_gather(share, 'ra', axis=1, tiled=True)  59.7 us
    psum x2, blocking collectives, body(): total = lax.psum(squares, 'ra')  22.2 us
    dot_general x2, matrix products, body(): jnp.dot(hidden, down_weight[layer], preferred_element_type=jnp.float32)  10.8 us
    dot_general x2, matrix products, body(): jnp.dot(normed, up_weight[layer], preferred_element_type=jnp.float32)  10.6 us
    dot_general x2, matrix products, body(): jnp.dot(normed, gate_weight[layer], preferred_element_type=jnp.float32)  10.2 us
  transfers between devices with their start and end apart: 8, of which 8 were waited for; matrix products, arithmetic and copies ran while one was open for 3% of the time, Pallas kernels for 0%

commit v1 on v0

--- a/solution.py
+++ b/solution.py
@@ -17,7 +17,7 @@
         normed = (widened * norm_gain[layer]).astype(jnp.bfloat16)
         gate_part = jnp.dot(normed, gate_weight[layer], preferred_element_type=jnp.float32)
         up_part = jnp.dot(normed, up_weight[layer], preferred_element_type=jnp.float32)
-        total = lax.psum(squares, "ra")
+        total = jnp.sum(lax.all_gather(squares, "ra"), axis=0)
         gate_share, up_share = (
             lax.psum_scatter(gate_part, "ra", scatter_dimension=1, tiled=True),
             lax.psum_scatter(up_part, "ra", scatter_dimension=1, tiled=True),

time: 412 us -> 412 us (level)
    psum x2 -> x0, blocking collectives: 22.2 us -> none  [body(): total = lax.psum(squares, 'ra')]
    all_gather x0 -> x2, blocking collectives: none -> 18.2 us  [body(): total = jnp.sum(lax.all_gather(squares, 'ra'), axis=0)]
where the time goes in v1:
time: 412 us; the launch traced here: 411 us
  waiting for transfers between devices  336 us (82%)
  matrix products  31.6 us (8%)
  blocking collectives  18.2 us (4%)
  between operations  13.5 us (3%)
  other arithmetic  9.85 us (2%)
    psum x2, waiting for transfers between devices, body(): branch = lax.psum(partial_down, 'cb')  130 us
    reduce_scatter x2, waiting for transfers between devices, body(): lax.psum_scatter(up_part, 'ra', scatter_dimension=1, tiled=True)  72.7 us
    reduce_scatter x2, waiting for transfers between devices, body(): lax.psum_scatter(gate_part, 'ra', scatter_dimension=1, tiled=True)  72.7 us
    all_gather x2, waiting for transfers between devices, body(): hidden = lax.all_gather(share, 'ra', axis=1, tiled=True)  59.7 us
    all_gather x2, blocking collectives, body(): total = jnp.sum(lax.all_gather(squares, 'ra'), axis=0)  18.2 us
    dot_general x2, matrix products, body(): jnp.dot(hidden, down_weight[layer], preferred_element_type=jnp.float32)  10.8 us
    dot_general x2, matrix products, body(): jnp.dot(normed, up_weight[layer], preferred_element_type=jnp.float32)  10.6 us
    dot_general x2, matrix products, body(): jnp.dot(normed, gate_weight[layer], preferred_element_type=jnp.float32)  10.2 us
  transfers between devices with their start and end apart: 8, of which 8 were waited for; matrix products, arithmetic and copies ran while one was open for 3% of the time, Pallas kernels for 0%

profile of v1, /device:TPU:0, one launch (start us, length us, event | category | flops | bytes accessed | tf_op | source)
XLA Modules:
  0.0 411.0 jit_solution(12829749652026865990)
XLA Ops:
  6.5 0.0 reduce-scatter.7.cloned.1.call-start
  6.5 0.8 fusion.31
  7.3 5.4 %fusion.8 = f32[512,1408]{0,1:T(8,128)} fusion(bf16[2,1024,1408]{2,1,0:T(8,128)(2,1)} %param.8, bf16[512,1024]{1,0:T(8,128)(2,1)} %param.5, f32[1024]{0:T(1024)S(1)} %bitcast.28), kind=kOutput, calls=%fused_computation.14 | convolution fusion | flops 1477967872 | bytes 6819840 | tf_op jit(solution)/shard_map/dot_general | solution.py:19
  12.7 0.0 copy-start
  12.7 0.0 reduce-scatter.7.cloned.1.call-update
  12.8 0.0 reduce-scatter.5.cloned.1.call-start
  12.8 1.1 copy-done
  14.0 5.1 %fusion.10 = f32[512,1408]{0,1:T(8,128)} fusion(bf16[2,1024,1408]{2,1,0:T(8,128)(2,1)} %param.7, bf16[512,1024]{1,0:T(8,128)(2,1)S(1)} %copy-done, f32[1024]{0:T(1024)S(1)} %bitcast.29), kind=kOutput, calls=%fused_computation.16 | convolution fusion | flops 1477967872 | bytes 6819840 | tf_op jit(solution)/shard_map/dot_general | solution.py:18
  19.1 0.0 reduce-scatter.5.cloned.1.call-update
  19.1 0.0 all-gather.7.cloned.1.call-start
  19.2 0.3 fusion.21
  19.5 9.9 %all-gather.2 = f32[4,1,512]{2,1,0:T(1,128)S(1)} all-gather(f32[1,1,512]{2,1,0:T(1,128)S(1)} %bitcast.25), channel_id=2, replica_groups=mesh['ra'=4,'cb'=8] {'ra'}, dimensions={0}, use_global_device_ids=true | all-gather | bytes 10240 | tf_op jit(solution)/shard_map/all_gather | solution.py:20
  29.4 28.1 %reduce-scatter.7.cloned.1.call-done = f32[512,352]{0,1:T(8,128)} async-done(((f32[512,1408]{0,1:T(8,128)}), f32[512,352]{0,1:T(8,128)}) %reduce-scatter.7.cloned.1.call-update) | async-done | bytes 720912 | tf_op jit(solution)/shard_map/reduce_scatter | solution.py:23
  57.4 44.8 %reduce-scatter.5.cloned.1.call-done = f32[512,352]{0,1:T(8,128)} async-done(((f32[512,1408]{0,1:T(8,128)}), f32[512,352]{0,1:T(8,128)}) %reduce-scatter.5.cloned.1.call-update) | async-done | bytes 720912 | tf_op jit(solution)/shard_map/reduce_scatter | solution.py:22
  102.3 2.3 multiply_convert_fusion.1
  104.5 0.0 all-gather.7.cloned.1.call-update
  104.6 0.0 all-reduce.3.cloned.1.call-start
  104.6 29.8 %all-gather.7.cloned.1.call-done = bf16[512,1408]{0,1:T(8,128)(2,1)} async-done(((bf16[512,352]{0,1:T(8,128)(2,1)}), bf16[512,1408]{0,1:T(8,128)(2,1)}) %all-gather.7.cloned.1.call-update) | async-done | bytes 1441808 | tf_op jit(solution)/shard_map/all_gather | solution.py:27
  134.4 5.4 %fusion.6 = f32[512,1024]{1,0:T(8,128)} fusion(bf16[512,1408]{0,1:T(8,128)(2,1)} %all-gather.7.cloned.1.call-done, bf16[2,1408,1024]{2,1,0:T(8,128)(2,1)} %param.9), kind=kOutput, calls=%fused_computation.12 | convolution fusion | flops 1476395008 | bytes 6422528 | tf_op jit(solution)/shard_map/dot_general | solution.py:28
  139.9 0.0 all-reduce.3.cloned.1.call-update
  139.9 0.0 reduce-scatter.9.cloned.1.call-start
  139.9 65.2 %all-reduce.3.cloned.1.call-done = f32[512,1024]{1,0:T(8,128)} async-done(((f32[512,1024]{1,0:T(8,128)}), f32[512,1024]{1,0:T(8,128)}) %all-reduce.3.cloned.1.call-update) | async-done | bytes 2097168 | tf_op jit(solution)/shard_map/psum | solution.py:29
  205.1 2.0 fusion.25
  207.1 5.1 %fusion.4 = f32[512,1408]{0,1:T(8,128)} fusion(bf16[2,1024,1408]{2,1,0:T(8,128)(2,1)} %param.7, bf16[512,1024]{1,0:T(8,128)(2,1)S(1)} %get-tuple-element.6, f32[1024]{0:T(1024)S(1)} %bitcast.26), kind=kOutput, calls=%fused_computation.10 | convolution fusion | flops 1477967872 | bytes 6819840 | tf_op jit(solution)/shard_map/dot_general | solution.py:18
  212.2 0.0 reduce-scatter.9.cloned.1.call-update
  212.2 0.0 reduce-scatter.11.cloned.1.call-start
  212.3 5.1 %fusion.2 = f32[512,1408]{0,1:T(8,128)} fusion(bf16[2,1024,1408]{2,1,0:T(8,128)(2,1)} %param.8, bf16[512,1024]{1,0:T(8,128)(2,1)S(1)} %get-tuple-element.6, f32[1024]{0:T(1024)S(1)} %bitcast.27), kind=kOutput, calls=%fused_computation.8 | convolution fusion | flops 1477967872 | bytes 6819840 | tf_op jit(solution)/shard_map/dot_general | solution.py:19
  217.4 0.0 reduce-scatter.11.cloned.1.call-update
  217.5 0.0 all-gather.9.cloned.1.call-start
  217.5 8.4 %all-gather.3 = f32[4,1,512]{2,1,0:T(1,128)S(1)} all-gather(f32[1,1,512]{2,1,0:T(1,128)S(1)} %bitcast.24), channel_id=3, replica_groups=mesh['ra'=4,'cb'=8] {'ra'}, dimensions={0}, use_global_device_ids=true | all-gather | bytes 10240 | tf_op jit(solution)/shard_map/all_gather | solution.py:20
  225.9 27.9 %reduce-scatter.9.cloned.1.call-done = f32[512,352]{0,1:T(8,128)} async-done(((f32[512,1408]{0,1:T(8,128)}), f32[512,352]{0,1:T(8,128)}) %reduce-scatter.9.cloned.1.call-update) | async-done | bytes 720912 | tf_op jit(solution)/shard_map/reduce_scatter | solution.py:22
  253.8 44.7 %reduce-scatter.11.cloned.1.call-done = f32[512,352]{0,1:T(8,128)} async-done(((f32[512,1408]{0,1:T(8,128)}), f32[512,352]{0,1:T(8,128)}) %reduce-scatter.11.cloned.1.call-update) | async-done | bytes 720912 | tf_op jit(solution)/shard_map/reduce_scatter | solution.py:23
  298.4 2.3 multiply_convert_fusion
  300.7 0.0 all-gather.9.cloned.1.call-update
  300.7 0.0 all-reduce.5.cloned.1.call-start
  300.8 29.9 %all-gather.9.cloned.1.call-done = bf16[512,1408]{0,1:T(8,128)(2,1)} async-done(((bf16[512,352]{0,1:T(8,128)(2,1)}), bf16[512,1408]{0,1:T(8,128)(2,1)}) %all-gather.9.cloned.1.call-update) | async-done | bytes 1441808 | tf_op jit(solution)/shard_map/all_gather | solution.py:27
  330.6 5.4 %fusion = f32[512,1024]{1,0:T(8,128)} fusion(bf16[512,1408]{0,1:T(8,128)(2,1)} %all-gather.9.cloned.1.call-done, bf16[2,1408,1024]{2,1,0:T(8,128)(2,1)} %param.9), kind=kOutput, calls=%fused_computation.6 | convolution fusion | flops 1476395008 | bytes 6422528 | tf_op jit(solution)/shard_map/dot_general | solution.py:28
  336.0 0.0 all-reduce.5.cloned.1.call-update
  336.1 65.2 %all-reduce.5.cloned.1.call-done = f32[512,1024]{1,0:T(8,128)} async-done(((f32[512,1024]{1,0:T(8,128)}), f32[512,1024]{1,0:T(8,128)}) %all-reduce.5.cloned.1.call-update) | async-done | bytes 2097168 | tf_op jit(solution)/shard_map/psum | solution.py:29
  401.3 2.9 fusion.23
  (4 shorter events, 0.1 us)
Async XLA Ops:
  6.5 50.9 %reduce-scatter.7.cloned.1.call-start = ((), (), s32[]{:S(2)}) async-start(), calls=%async_computation.5 | async-start | bytes 3604480 | tf_op jit(solution)/shard_map/reduce_scatter | solution.py:23
  12.7 1.2 copy-start
  12.8 89.5 %reduce-scatter.5.cloned.1.call-start = ((), (), s32[]{:S(2)}) async-start(), calls=%async_computation.4 | async-start | bytes 3604480 | tf_op jit(solution)/shard_map/reduce_scatter | solution.py:22
  19.1 115.3 %all-gather.7.cloned.1.call-start = ((), (), s32[]{:S(2)}) async-start(), calls=%async_computation.6 | async-start | bytes 1802240 | tf_op jit(solution)/shard_map/all_gather | solution.py:27
  104.6 100.5 %all-reduce.3.cloned.1.call-start = ((), (), s32[]{:S(2)}) async-start(), calls=%async_computation.7 | async-start | bytes 4194304 | tf_op jit(solution)/shard_map/psum | solution.py:29
  139.9 113.9 %reduce-scatter.9.cloned.1.call-start = ((), (), s32[]{:S(2)}) async-start(), calls=%async_computation.8 | async-start | bytes 3604480 | tf_op jit(solution)/shard_map/reduce_scatter | solution.py:22
  212.2 86.2 %reduce-scatter.11.cloned.1.call-start = ((), (), s32[]{:S(2)}) async-start(), calls=%async_computation.9 | async-start | bytes 3604480 | tf_op jit(solution)/shard_map/reduce_scatter | solution.py:23
  217.5 113.2 %all-gather.9.cloned.1.call-start = ((), (), s32[]{:S(2)}) async-start(), calls=%async_computation.10 | async-start | bytes 1802240 | tf_op jit(solution)/shard_map/all_gather | solution.py:27
  300.7 100.6 %all-reduce.5.cloned.1.call-start = ((), (), s32[]{:S(2)}) async-start(), calls=%async_computation.11 | async-start | bytes 4194304 | tf_op jit(solution)/shard_map/psum | solution.py:29
Sparse Core Ops, SparseCore 0:
  12.9 44.5 reduce-scatter.6
  60.5 41.7 reduce-scatter.4
  104.7 29.7 all-gather.6
  140.0 65.0 all-reduce.2
  212.4 41.3 reduce-scatter.8
  256.7 41.7 reduce-scatter.10
  300.8 29.7 all-gather.8
  336.2 65.0 all-reduce.4
